TPU v7x, 32 devices: a whole 2x2x4 slice. The times are simulated.
32 devices in a mesh: rep: 2 (over x), fs: 8 (over z, y), tp: 2 (over core).
Axes of the slice: x: 2, y: 2, z: 4, core: 2. Of those that a mesh axis runs over, the one named last changes fastest.
Arguments:
- tokens: bfloat16 [8192, 2048], P(('rep', 'fs')), may hold values from -6 to 6
- mix_gain: bfloat16 [2048], replicated, may hold values from 0.099609375 to 1.8984375
- value_weight: bfloat16 [2048, 1536], P('fs', 'tp'), may hold values from -0.125 to 0.125
- outer_gate_weight: bfloat16 [2048, 1536], P('fs', 'tp'), may hold values from -0.125 to 0.125
- inner_gate_weight: bfloat16 [2048, 1536], P('fs', 'tp'), may hold values from -0.125 to 0.125
- conv_taps: bfloat16 [3, 1536], P(None, 'tp'), may hold values from -3 to 3
- mix_out_weight: bfloat16 [1536, 2048], P('tp', 'fs'), may hold values from -0.15625 to 0.15625
- ffn_gain: bfloat16 [2048], replicated, may hold values from 0.099609375 to 1.8984375
- gate_weight: bfloat16 [2048, 4096], P('fs', 'tp'), may hold values from -0.125 to 0.125
- up_weight: bfloat16 [2048, 4096], P('fs', 'tp'), may hold values from -0.125 to 0.125
- down_weight: bfloat16 [4096, 2048], P('tp', 'fs'), may hold values from -0.09375 to 0.09375
Outputs:
- layer_out: bfloat16 [8192, 2048], P(('rep', 'fs'))
All inputs are finite; a program needn't handle non-finite values.
Results may differ from a plain program's by a relative error of at most 0.02.
Values may be sent and summed in bfloat16 or wider, within the bound.
A program may use at most 128 MiB of HBM per device.

v0:
```python
import jax
import jax.numpy as jnp
from jax import lax
from jax.sharding import PartitionSpec as P

SEQ_GRP = 2
EPS = 1e-05


def rms_norm(values, gain):
    floats = values.astype(jnp.float32)
    scaled = floats * lax.rsqrt(jnp.mean(floats * floats, axis=-1, keepdims=True) + EPS)
    return (scaled * gain.astype(jnp.float32)).astype(jnp.bfloat16)


def short_conv(value_proj, outer_proj, inner_proj, conv_taps, seq_len):
    mixed_in = inner_proj.astype(jnp.float32) * value_proj.astype(jnp.float32)
    count_rows = mixed_in.shape[0]
    position = (jnp.arange(count_rows, dtype=jnp.int32) % seq_len)[:, None]
    zero_row = jnp.zeros((1, mixed_in.shape[1]), jnp.float32)
    back_one = jnp.where(position >= 1, jnp.concatenate([zero_row, mixed_in[:-1]], axis=0), 0.0)
    back_two = jnp.where(
        position >= 2, jnp.concatenate([zero_row, zero_row, mixed_in[:-2]], axis=0), 0.0
    )
    taps = conv_taps.astype(jnp.float32)
    convolved = taps[0] * back_two + taps[1] * back_one + taps[2] * mixed_in
    return (outer_proj.astype(jnp.float32) * convolved).astype(jnp.bfloat16)


def local(
    tokens,
    mix_gain,
    value_weight,
    outer_gate_weight,
    inner_gate_weight,
    conv_taps,
    mix_out_weight,
    ffn_gain,
    gate_weight,
    up_weight,
    down_weight,
):
    row_count = tokens.shape[0]
    share = row_count // lax.axis_size("tp")
    seq_len = row_count // SEQ_GRP
    own_rows = lax.dynamic_slice_in_dim(tokens, lax.axis_index("tp") * share, share, 0).astype(
        jnp.float32
    )
    normed = rms_norm(tokens, mix_gain)
    value_full, outer_full, inner_full, mix_out_full, gate_full, up_full, down_full = (
        lax.all_gather(value_weight, "fs", axis=0, tiled=True),
        lax.all_gather(outer_gate_weight, "fs", axis=0, tiled=True),
        lax.all_gather(inner_gate_weight, "fs", axis=0, tiled=True),
        lax.all_gather(mix_out_weight, "fs", axis=1, tiled=True),
        lax.all_gather(gate_weight, "fs", axis=0, tiled=True),
        lax.all_gather(up_weight, "fs", axis=0, tiled=True),
        lax.all_gather(down_weight, "fs", axis=1, tiled=True),
    )
    value_proj = jnp.dot(normed, value_full, preferred_element_type=jnp.float32).astype(
        jnp.bfloat16
    )
    outer_proj = jnp.dot(normed, outer_full, preferred_element_type=jnp.float32).astype(
        jnp.bfloat16
    )
    inner_proj = jnp.dot(normed, inner_full, preferred_element_type=jnp.float32).astype(
        jnp.bfloat16
    )
    mixed = short_conv(value_proj, outer_proj, inner_proj, conv_taps, seq_len)
    picked = mixed
    mix_total = lax.psum_scatter(
        jnp.dot(picked, mix_out_full, preferred_element_type=jnp.float32).astype(jnp.bfloat16),
        "tp",
        scatter_dimension=0,
        tiled=True,
    ).astype(jnp.float32)
    after_mix = (own_rows + mix_total).astype(jnp.bfloat16)
    normed_two = rms_norm(after_mix, ffn_gain)
    block_rows = lax.all_gather(normed_two, "tp", axis=0, tiled=True)
    gate_proj = jnp.dot(block_rows, gate_full, preferred_element_type=jnp.float32)
    up_proj = jnp.dot(block_rows, up_full, preferred_element_type=jnp.float32)
    hidden = (jax.nn.silu(gate_proj) * up_proj).astype(jnp.bfloat16)
    picked = hidden
    ffn_total = lax.psum_scatter(
        jnp.dot(picked, down_full, preferred_element_type=jnp.float32).astype(jnp.bfloat16),
        "tp",
        scatter_dimension=0,
        tiled=True,
    ).astype(jnp.float32)
    finished = (after_mix.astype(jnp.float32) + ffn_total).astype(jnp.bfloat16)
    return lax.all_gather(finished, "tp", axis=0, tiled=True)


def solution(mesh):
    placed = (
        P(("rep", "fs"), None),
        P(),
        P("fs", "tp"),
        P("fs", "tp"),
        P("fs", "tp"),
        P(None, "tp"),
        P("tp", "fs"),
        P(),
        P("fs", "tp"),
        P("fs", "tp"),
        P("tp", "fs"),
    )
    return jax.shard_map(
        local, mesh=mesh, in_specs=placed, out_specs=P(("rep", "fs"), None), check_vma=False
    )
```

profile of v0, /device:TPU:0, one launch (start us, length us, event | category | flops | bytes accessed | tf_op | source)
XLA Modules:
  0.0 718.0 jit_solution(16249208888733937228)
XLA Ops:
  6.5 0.7 all-gather.14.cloned.1.call-update
  7.3 0.7 all-gather.12.cloned.1.call-update
  8.1 0.7 all-gather.10.cloned.1.call-update
  8.8 0.5 all-gather.16.cloned.1.call-update
  9.4 0.7 convert_element_type.69
  10.1 0.7 convert_element_type.73
  10.8 2.1 fusion
  12.9 59.4 %all-gather.14.cloned.1.call-done = bf16[2048,768]{1,0:T(8,128)(2,1)} async-done(((bf16[256,768]{1,0:T(8,128)(2,1)}), bf16[2048,768]{1,0:T(8,128)(2,1)}) %all-gather.14.cloned.1.call-update) | async-done | bytes 3145744 | tf_op jit(solution)/shard_map/all_gather | solution.py:51
  72.3 3.7 convolution_convert_fusion.2
  76.0 57.2 %all-gather.12.cloned.1.call-done = bf16[2048,768]{1,0:T(8,128)(2,1)} async-done(((bf16[256,768]{1,0:T(8,128)(2,1)}), bf16[2048,768]{1,0:T(8,128)(2,1)}) %all-gather.12.cloned.1.call-update) | async-done | bytes 3145744 | tf_op jit(solution)/shard_map/all_gather | solution.py:53
  133.2 4.9 convert_multiply_fusion.4
  138.1 56.0 %all-gather.10.cloned.1.call-done = bf16[2048,768]{1,0:T(8,128)(2,1)} async-done(((bf16[256,768]{1,0:T(8,128)(2,1)}), bf16[2048,768]{1,0:T(8,128)(2,1)}) %all-gather.10.cloned.1.call-update) | async-done | bytes 3145744 | tf_op jit(solution)/shard_map/all_gather | solution.py:52
  194.1 63.2 %all-gather.16.cloned.1.call-done = bf16[768,2048]{1,0:T(8,128)(2,1)} async-done(((bf16[768,256]{1,0:T(8,128)(2,1)}), bf16[768,2048]{1,0:T(8,128)(2,1)}) %all-gather.16.cloned.1.call-update) | async-done | bytes 3145744 | tf_op jit(solution)/shard_map/all_gather | solution.py:54
  257.3 9.8 %convolution_convert_fusion.1 = bf16[512,2048]{1,0:T(8,128)(2,1)} fusion(bf16[768,2048]{1,0:T(8,128)(2,1)} %all-gather.16.cloned.1.call-done, f32[512,768]{1,0:T(8,128)} %convert_multiply_fusion.4, f32[511,768]{1,0:T(8,128)} %bitcast.20, f32[510,768]{1,0:T(8,128)} %bitcast.21, bf16[2048,768]{1,0:T(8,128)(2,1)} %all-gather.10.cloned.1.call-done, ...), kind=kOutput, calls=%fused_computation.10 | convolution fusion | flops 3230793728 | bytes 15215616 | tf_op jit(solution)/shard_map/dot_general | solution.py:71
  267.2 0.6 copy-done.1
  267.8 7.4 %reduce-scatter.3.cloned.1.call-done = bf16[256,2048]{1,0:T(8,128)(2,1)} async-done(((bf16[512,2048]{1,0:T(8,128)(2,1)}), bf16[256,2048]{1,0:T(8,128)(2,1)}) %reduce-scatter.3.cloned.1.call-update) | async-done | bytes 1048592 | tf_op jit(solution)/shard_map/reduce_scatter | solution.py:70
  275.3 1.7 fusion.3
  277.0 1.3 fusion.5
  278.4 0.7 all-gather.20.cloned.1.call-update
  279.1 0.7 all-gather.22.cloned.1.call-update
  279.9 0.7 all-gather.24.cloned.1.call-update
  280.6 0.2 reduce-scatter.5.cloned.1.call-start
  280.8 9.6 %all-gather.18.cloned.1.call-done = bf16[512,2048]{1,0:T(8,128)(2,1)} async-done(((bf16[256,2048]{1,0:T(8,128)(2,1)}), bf16[512,2048]{1,0:T(8,128)(2,1)}) %all-gather.18.cloned.1.call-update) | async-done | bytes 2097168 | tf_op jit(solution)/shard_map/all_gather | solution.py:78
  290.4 127.8 %all-gather.20.cloned.1.call-done = bf16[2048,2048]{1,0:T(8,128)(2,1)} async-done(((bf16[256,2048]{1,0:T(8,128)(2,1)}), bf16[2048,2048]{1,0:T(8,128)(2,1)}) %all-gather.20.cloned.1.call-update) | async-done | bytes 8388624 | tf_op jit(solution)/shard_map/all_gather | solution.py:55
  418.2 10.5 %fusion.17 = f32[512,2048]{1,0:T(8,128)} fusion(bf16[512,2048]{1,0:T(8,128)(2,1)} %all-gather.18.cloned.1.call-done, bf16[2048,2048]{1,0:T(8,128)(2,1)} %all-gather.20.cloned.1.call-done), kind=kOutput, calls=%fused_computation.34 | convolution fusion | flops 4294967296 | bytes 14680064 | tf_op jit(solution)/shard_map/dot_general | solution.py:79
  428.6 114.3 %all-gather.22.cloned.1.call-done = bf16[2048,2048]{1,0:T(8,128)(2,1)} async-done(((bf16[256,2048]{1,0:T(8,128)(2,1)}), bf16[2048,2048]{1,0:T(8,128)(2,1)}) %all-gather.22.cloned.1.call-update) | async-done | bytes 8388624 | tf_op jit(solution)/shard_map/all_gather | solution.py:56
  543.0 125.2 %all-gather.24.cloned.1.call-done = bf16[2048,2048]{1,0:T(8,128)(2,1)} async-done(((bf16[2048,256]{1,0:T(8,128)(2,1)}), bf16[2048,2048]{1,0:T(8,128)(2,1)}) %all-gather.24.cloned.1.call-update) | async-done | bytes 8388624 | tf_op jit(solution)/shard_map/all_gather | solution.py:57
  668.2 17.4 %convolution_convert_fusion = bf16[512,2048]{1,0:T(8,128)(2,1)} fusion(bf16[2048,2048]{1,0:T(8,128)(2,1)} %all-gather.24.cloned.1.call-done, f32[512,2048]{1,0:T(8,128)} %fusion.17, bf16[512,2048]{1,0:T(8,128)(2,1)S(1)} %copy-done.2, bf16[2048,2048]{1,0:T(8,128)(2,1)} %all-gather.22.cloned.1.call-done), kind=kOutput, calls=%fused_computation.9 | convolution fusion | flops 8597274624 | bytes 25165824 | tf_op jit(solution)/shard_map/dot_general | solution.py:84
  685.7 8.0 %reduce-scatter.5.cloned.1.call-done = bf16[256,2048]{1,0:T(8,128)(2,1)} async-done(((bf16[512,2048]{1,0:T(8,128)(2,1)}), bf16[256,2048]{1,0:T(8,128)(2,1)}) %reduce-scatter.5.cloned.1.call-update) | async-done | bytes 1048592 | tf_op jit(solution)/shard_map/reduce_scatter | solution.py:83
  693.7 2.6 fusion.6
  696.3 12.0 %all-gather.26.cloned.1.call-done = bf16[512,2048]{1,0:T(8,128)(2,1)} async-done(((bf16[256,2048]{1,0:T(8,128)(2,1)}), bf16[512,2048]{1,0:T(8,128)(2,1)}) %all-gather.26.cloned.1.call-update) | async-done | bytes 2097168 | tf_op jit(solution)/shard_map/all_gather | solution.py:90
  708.3 3.2 copy.13
  (24 shorter events, 0.5 us)
Async XLA Ops:
  6.5 65.8 %copy-start = (bf16[512,2048]{1,0:T(8,128)(2,1)S(1)}, bf16[512,2048]{1,0:T(8,128)(2,1)}, u32[]{:S(2)}) copy-start(bf16[512,2048]{1,0:T(8,128)(2,1)} %param.11) | copy-start | bytes 6291460
  6.5 65.8 %all-gather.14.cloned.1.call-start = ((), (), s32[]{:S(2)}) async-start(), calls=%async_computation.4 | async-start | bytes 3538944 | tf_op jit(solution)/shard_map/all_gather | solution.py:51
  7.3 125.9 %all-gather.12.cloned.1.call-start = ((), (), s32[]{:S(2)}) async-start(), calls=%async_computation.3 | async-start | bytes 3538944 | tf_op jit(solution)/shard_map/all_gather | solution.py:53
  8.0 186.1 %all-gather.10.cloned.1.call-start = ((), (), s32[]{:S(2)}) async-start(), calls=%async_computation.2 | async-start | bytes 3538944 | tf_op jit(solution)/shard_map/all_gather | solution.py:52
  8.7 248.6 %all-gather.16.cloned.1.call-start = ((), (), s32[]{:S(2)}) async-start(), calls=%async_computation.5 | async-start | bytes 3538944 | tf_op jit(solution)/shard_map/all_gather | solution.py:54
  9.3 266.0 %reduce-scatter.3.cloned.1.call-start = ((), (), s32[]{:S(2)}) async-start(), calls=%async_computation.6 | async-start | bytes 3145728 | tf_op jit(solution)/shard_map/reduce_scatter | solution.py:70
  267.2 0.7 copy-start.1
  267.2 23.2 %all-gather.18.cloned.1.call-start = ((), (), s32[]{:S(2)}) async-start(), calls=%async_computation.7 | async-start | bytes 3145728 | tf_op jit(solution)/shard_map/all_gather | solution.py:78
  278.3 139.8 %all-gather.20.cloned.1.call-start = ((), (), s32[]{:S(2)}) async-start(), calls=%async_computation.8 | async-start | bytes 9437184 | tf_op jit(solution)/shard_map/all_gather | solution.py:55
  279.1 263.9 %all-gather.22.cloned.1.call-start = ((), (), s32[]{:S(2)}) async-start(), calls=%async_computation.9 | async-start | bytes 9437184 | tf_op jit(solution)/shard_map/all_gather | solution.py:56
  279.8 388.3 %all-gather.24.cloned.1.call-start = ((), (), s32[]{:S(2)}) async-start(), calls=%async_computation.10 | async-start | bytes 9437184 | tf_op jit(solution)/shard_map/all_gather | solution.py:57
  280.6 413.1 %reduce-scatter.5.cloned.1.call-start = ((), (), s32[]{:S(2)}) async-start(), calls=%async_computation.11 | async-start | bytes 3145728 | tf_op jit(solution)/shard_map/reduce_scatter | solution.py:83
  290.4 377.8 %copy-start.2 = (bf16[512,2048]{1,0:T(8,128)(2,1)S(1)}, bf16[512,2048]{1,0:T(8,128)(2,1)}, u32[]{:S(2)}) copy-start(bf16[512,2048]{1,0:T(8,128)(2,1)} %all-gather.18.cloned.1.call-done) | copy-start | bytes 6291460
  685.6 22.7 %all-gather.26.cloned.1.call-start = ((), (), s32[]{:S(2)}) async-start(), calls=%async_computation.12 | async-start | bytes 3145728 | tf_op jit(solution)/shard_map/all_gather | solution.py:90
Sparse Core Ops, SparseCore 0:
  9.5 62.7 all-gather.13
  74.5 58.6 all-gather.11
  135.4 58.6 all-gather.9
  196.0 61.3 all-gather.15
  267.3 7.9 reduce-scatter.2
  278.5 11.8 all-gather.17
  292.5 125.6 all-gather.19
  420.3 122.6 all-gather.21
  545.0 123.1 all-gather.23
  685.7 7.9 reduce-scatter.4
  696.4 11.8 all-gather.25
where the time goes:
time: 718 us
  waiting for transfers between devices  645 us (90%)
  matrix products  46.3 us (6%)
  between operations  13.3 us (2%)
  other arithmetic  9.09 us (1%)
    all_gather x1, waiting for transfers between devices, local(): lax.all_gather(gate_weight, 'fs', axis=0, tiled=True)  128 us
    all_gather x1, waiting for transfers between devices, local(): lax.all_gather(down_weight, 'fs', axis=1, tiled=True)  125 us
    all_gather x1, waiting for transfers between devices, local(): lax.all_gather(up_weight, 'fs', axis=0, tiled=True)  114 us
    all_gather x1, waiting for transfers between devices, local(): lax.all_gather(mix_out_weight, 'fs', axis=1, tiled=True)  63.2 us
    all_gather x1, waiting for transfers between devices, local(): lax.all_gather(value_weight, 'fs', axis=0, tiled=True)  59.4 us
    all_gather x1, waiting for transfers between devices, local(): lax.all_gather(inner_gate_weight, 'fs', axis=0, tiled=True)  57.2 us
    all_gather x1, waiting for transfers between devices, local(): lax.all_gather(outer_gate_weight, 'fs', axis=0, tiled=True)  56 us
    dot_general x1, matrix products, local(): jnp.dot(picked, down_full, preferred_element_type=jnp.float32)  17.4 us
  transfers between devices with their start and end apart: 11, of which 11 were waited for; matrix products, arithmetic and copies ran while one was open for 3% of the time, Pallas kernels for 0%

commit v1 on v0

--- a/solution.py
+++ b/solution.py
@@ -5,6 +5,28 @@
 
 SEQ_GRP = 2
 EPS = 1e-05
+
+
+def laid_out(tiles, dim):
+    tiles = jnp.moveaxis(tiles, 0, dim)
+    dims = tiles.shape
+    return tiles.reshape(*dims[:dim], dims[dim] * dims[dim + 1], *dims[dim + 2 :])
+
+
+def collect(array, axis, dim):
+    devices = lax.axis_size(axis)
+    pairs = [(i, (i + 1) % devices) for i in range(devices)]
+    back = [(b, a) for a, b in pairs]
+    lower, upper = ([], [])
+    for step in range(devices - 1):
+        if step % 2 == 0:
+            lower.append(lax.ppermute(lower[-1] if lower else array, axis, pairs))
+        else:
+            upper.append(lax.ppermute(upper[-1] if upper else array, axis, back))
+    pieces = jnp.stack([*lower[::-1], array, *upper])
+    shift = lax.axis_index(axis) - len(lower)
+    pieces = pieces[(jnp.arange(devices) - shift) % devices]
+    return laid_out(pieces, dim)
 
 
 def rms_norm(values, gain):
@@ -50,7 +72,7 @@
     value_full, outer_full, inner_full, mix_out_full, gate_full, up_full, down_full = (
         lax.all_gather(value_weight, "fs", axis=0, tiled=True),
         lax.all_gather(outer_gate_weight, "fs", axis=0, tiled=True),
-        lax.all_gather(inner_gate_weight, "fs", axis=0, tiled=True),
+        collect(inner_gate_weight, "fs", 0),
         lax.all_gather(mix_out_weight, "fs", axis=1, tiled=True),
         lax.all_gather(gate_weight, "fs", axis=0, tiled=True),
         lax.all_gather(up_weight, "fs", axis=0, tiled=True),

time: 718 us -> 696 us (0.969)
  waiting for transfers between devices: 645 us -> 599 us
  starting transfers between devices: 0.57 us -> 16.9 us
  local copies, waits for them, and re-layouts: 3.81 us -> 13.9 us
    ppermute x0 -> x7, waiting for transfers between devices: none -> 68.8 us  [the longest x4 61 us: collect(): lower.append(lax.ppermute(lower[-1] if lower else array, axis, pairs))]
    all_gather x1 -> x0, waiting for transfers between devices: 57.2 us -> none  [local(): lax.all_gather(inner_gate_weight, 'fs', axis=0, tiled=True)]
    all_gather x1, waiting for transfers between devices: 59.4 us -> 2.43 us  [local(): lax.all_gather(value_weight, 'fs', axis=0, tiled=True)]
    ppermute x0 -> x7, starting transfers between devices: none -> 16.4 us  [the longest x3 10.9 us: collect(): upper.append(lax.ppermute(upper[-1] if upper else array, axis, back))]
  transfers between devices with their start and end apart: 11 -> 17, of which waited for: 11 -> 15; matrix products, arithmetic and copies ran while one was open for 3% -> 4% of each run, Pallas kernels for 0% -> 0%
where the time goes in v1:
time: 696 us; the launch traced here: 695 us
  waiting for transfers between devices  599 us (86%)
  matrix products  44.6 us (6%)
  starting transfers between devices  16.9 us (2%)
  local copies, waits for them, and re-layouts  13.9 us (2%)
  between operations  13.6 us (2%)
  other arithmetic  7.73 us (1%)
    all_gather x1, waiting for transfers between devices, local(): lax.all_gather(gate_weight, 'fs', axis=0, tiled=True)  128 us
    all_gather x1, waiting for transfers between devices, local(): lax.all_gather(down_weight, 'fs', axis=1, tiled=True)  125 us
    all_gather x1, waiting for transfers between devices, local(): lax.all_gather(up_weight, 'fs', axis=0, tiled=True)  114 us
    ppermute x4, waiting for transfers between devices, collect(): lower.append(lax.ppermute(lower[-1] if lower else array, axis, pairs))  61 us
    all_gather x1, waiting for transfers between devices, local(): lax.all_gather(outer_gate_weight, 'fs', axis=0, tiled=True)  60.4 us
    all_gather x1, waiting for transfers between devices, local(): lax.all_gather(mix_out_weight, 'fs', axis=1, tiled=True)  57.4 us
    dot_general x1, matrix products, local(): jnp.dot(picked, down_full, preferred_element_type=jnp.float32)  17.4 us
  transfers between devices with their start and end apart: 17, of which 15 were waited for; matrix products, arithmetic and copies ran while one was open for 4% of the time, Pallas kernels for 0%

profile of v1, /device:TPU:0, one launch (start us, length us, event | category | flops | bytes accessed | tf_op | source)
XLA Modules:
  0.0 695.4 jit_solution(5265804674140308043)
XLA Ops:
  8.8 3.0 collective-permute-start
  11.8 12.5 %collective-permute-done = bf16[256,768]{1,0:T(8,128)(2,1)S(1)} collective-permute-done((bf16[256,768]{1,0:T(8,128)(2,1)}, bf16[256,768]{1,0:T(8,128)(2,1)S(1)}, u32[]{:S(2)}, u32[]{:S(2)}) %collective-permute-start) | collective-permute-done | bytes 393248 | tf_op jit(solution)/shard_map/ppermute | solution.py:23
  24.3 4.7 collective-permute-start.4
  29.0 17.7 %collective-permute-done.1 = bf16[256,768]{1,0:T(8,128)(2,1)S(1)} collective-permute-done((bf16[256,768]{1,0:T(8,128)(2,1)S(1)}, bf16[256,768]{1,0:T(8,128)(2,1)S(1)}, u32[]{:S(2)}, u32[]{:S(2)}) %collective-permute-start.1) | collective-permute-done | bytes 393248 | tf_op jit(solution)/shard_map/ppermute | solution.py:23
  46.8 2.1 fusion
  48.9 4.8 collective-permute-start.5
  53.7 18.2 %collective-permute-done.2 = bf16[256,768]{1,0:T(8,128)(2,1)S(1)} collective-permute-done((bf16[256,768]{1,0:T(8,128)(2,1)S(1)}, bf16[256,768]{1,0:T(8,128)(2,1)S(1)}, u32[]{:S(2)}, u32[]{:S(2)}) %collective-permute-start.2) | collective-permute-done | bytes 393248 | tf_op jit(solution)/shard_map/ppermute | solution.py:23
  71.8 2.5 collective-permute-start.3
  74.4 7.8 %collective-permute-done.5 = bf16[256,768]{1,0:T(8,128)(2,1)S(1)} collective-permute-done((bf16[256,768]{1,0:T(8,128)(2,1)S(1)}, bf16[256,768]{1,0:T(8,128)(2,1)S(1)}, u32[]{:S(2)}, u32[]{:S(2)}) %collective-permute-start.5) | collective-permute-done | bytes 393248 | tf_op jit(solution)/shard_map/ppermute | solution.py:25
  82.2 1.4 collective-permute-start.6
  83.6 12.6 %collective-permute-done.3 = bf16[256,768]{1,0:T(8,128)(2,1)S(1)} collective-permute-done((bf16[256,768]{1,0:T(8,128)(2,1)S(1)}, bf16[256,768]{1,0:T(8,128)(2,1)S(1)}, u32[]{:S(2)}, u32[]{:S(2)}) %collective-permute-start.3) | collective-permute-done | bytes 393248 | tf_op jit(solution)/shard_map/ppermute | solution.py:23
  96.2 0.8 bitcast_dynamic-update-slice_fusion.7
  102.5 4.4 gather_fusion
  107.0 2.4 all-gather.11.cloned.1.call-done
  109.4 3.9 convolution_convert_fusion.2
  113.3 3.1 convert_multiply_fusion.4
  116.4 57.4 %all-gather.13.cloned.1.call-done = bf16[768,2048]{1,0:T(8,128)(2,1)} async-done(((bf16[768,256]{1,0:T(8,128)(2,1)}), bf16[768,2048]{1,0:T(8,128)(2,1)}) %all-gather.13.cloned.1.call-update) | async-done | bytes 3145744 | tf_op jit(solution)/shard_map/all_gather | solution.py:76
  173.8 60.4 %all-gather.9.cloned.1.call-done = bf16[2048,768]{1,0:T(8,128)(2,1)} async-done(((bf16[256,768]{1,0:T(8,128)(2,1)}), bf16[2048,768]{1,0:T(8,128)(2,1)}) %all-gather.9.cloned.1.call-update) | async-done | bytes 3145744 | tf_op jit(solution)/shard_map/all_gather | solution.py:74
  234.2 9.8 %convolution_convert_fusion.1 = bf16[512,2048]{1,0:T(8,128)(2,1)} fusion(bf16[768,2048]{1,0:T(8,128)(2,1)} %all-gather.13.cloned.1.call-done, f32[512,768]{1,0:T(8,128)} %convert_multiply_fusion.4, f32[511,768]{1,0:T(8,128)} %bitcast.40, f32[510,768]{1,0:T(8,128)} %bitcast.41, bf16[2048,768]{1,0:T(8,128)(2,1)} %all-gather.9.cloned.1.call-done, ...), kind=kOutput, calls=%fused_computation.11 | convolution fusion | flops 3230793728 | bytes 15215616 | tf_op jit(solution)/shard_map/dot_general | solution.py:93
  244.1 8.5 %reduce-scatter.3.cloned.1.call-done = bf16[256,2048]{1,0:T(8,128)(2,1)} async-done(((bf16[512,2048]{1,0:T(8,128)(2,1)}), bf16[256,2048]{1,0:T(8,128)(2,1)}) %reduce-scatter.3.cloned.1.call-update) | async-done | bytes 1048592 | tf_op jit(solution)/shard_map/reduce_scatter | solution.py:92
  252.6 1.7 fusion.3
  254.3 1.3 fusion.5
  257.9 9.7 %all-gather.15.cloned.1.call-done = bf16[512,2048]{1,0:T(8,128)(2,1)} async-done(((bf16[256,2048]{1,0:T(8,128)(2,1)}), bf16[512,2048]{1,0:T(8,128)(2,1)}) %all-gather.15.cloned.1.call-update) | async-done | bytes 2097168 | tf_op jit(solution)/shard_map/all_gather | solution.py:100
  267.6 127.7 %all-gather.17.cloned.1.call-done = bf16[2048,2048]{1,0:T(8,128)(2,1)} async-done(((bf16[256,2048]{1,0:T(8,128)(2,1)}), bf16[2048,2048]{1,0:T(8,128)(2,1)}) %all-gather.17.cloned.1.call-update) | async-done | bytes 8388624 | tf_op jit(solution)/shard_map/all_gather | solution.py:77
  395.3 10.5 %fusion.19 = f32[512,2048]{1,0:T(8,128)} fusion(bf16[512,2048]{1,0:T(8,128)(2,1)} %all-gather.15.cloned.1.call-done, bf16[2048,2048]{1,0:T(8,128)(2,1)} %all-gather.17.cloned.1.call-done), kind=kOutput, calls=%fused_computation.50 | convolution fusion | flops 4294967296 | bytes 14680064 | tf_op jit(solution)/shard_map/dot_general | solution.py:101
  405.8 114.3 %all-gather.19.cloned.1.call-done = bf16[2048,2048]{1,0:T(8,128)(2,1)} async-done(((bf16[256,2048]{1,0:T(8,128)(2,1)}), bf16[2048,2048]{1,0:T(8,128)(2,1)}) %all-gather.19.cloned.1.call-update) | async-done | bytes 8388624 | tf_op jit(solution)/shard_map/all_gather | solution.py:78
  520.1 125.2 %all-gather.21.cloned.1.call-done = bf16[2048,2048]{1,0:T(8,128)(2,1)} async-done(((bf16[2048,256]{1,0:T(8,128)(2,1)}), bf16[2048,2048]{1,0:T(8,128)(2,1)}) %all-gather.21.cloned.1.call-update) | async-done | bytes 8388624 | tf_op jit(solution)/shard_map/all_gather | solution.py:79
  645.3 17.4 %convolution_convert_fusion = bf16[512,2048]{1,0:T(8,128)(2,1)} fusion(bf16[2048,2048]{1,0:T(8,128)(2,1)} %all-gather.21.cloned.1.call-done, f32[512,2048]{1,0:T(8,128)} %fusion.19, bf16[512,2048]{1,0:T(8,128)(2,1)S(1)} %copy-done.6, bf16[2048,2048]{1,0:T(8,128)(2,1)} %all-gather.19.cloned.1.call-done), kind=kOutput, calls=%fused_computation.10 | convolution fusion | flops 8597274624 | bytes 25165824 | tf_op jit(solution)/shard_map/dot_general | solution.py:106
  662.8 8.0 %reduce-scatter.5.cloned.1.call-done = bf16[256,2048]{1,0:T(8,128)(2,1)} async-done(((bf16[512,2048]{1,0:T(8,128)(2,1)}), bf16[256,2048]{1,0:T(8,128)(2,1)}) %reduce-scatter.5.cloned.1.call-update) | async-done | bytes 1048592 | tf_op jit(solution)/shard_map/reduce_scatter | solution.py:105
  670.8 2.6 fusion.6
  673.4 12.0 %all-gather.23.cloned.1.call-done = bf16[512,2048]{1,0:T(8,128)(2,1)} async-done(((bf16[256,2048]{1,0:T(8,128)(2,1)}), bf16[512,2048]{1,0:T(8,128)(2,1)}) %all-gather.23.cloned.1.call-update) | async-done | bytes 2097168 | tf_op jit(solution)/shard_map/all_gather | solution.py:112
  685.5 3.2 copy.20
  (54 shorter events, 10.2 us)
Async XLA Ops:
  6.5 67.8 %copy-start.4 = (bf16[2048]{0:T(1024)(128)(2,1)S(1)}, bf16[2048]{0:T(1024)(128)(2,1)}, u32[]{:S(2)}) copy-start(bf16[2048]{0:T(1024)(128)(2,1)} %param.12) | copy-start | bytes 12292
  6.5 67.8 %copy-start.3 = (bf16[3,768]{1,0:T(4,128)(2,1)S(1)}, bf16[3,768]{1,0:T(4,128)(2,1)}, u32[]{:S(2)}) copy-start(bf16[3,768]{1,0:T(4,128)(2,1)} %param.16) | copy-start | bytes 13828
  6.5 102.9 %all-gather.11.cloned.1.call-start = ((), (), s32[]{:S(2)}) async-start(), calls=%async_computation.3 | async-start | bytes 3538944 | tf_op jit(solution)/shard_map/all_gather | solution.py:73
  7.3 92.1 %copy-start.2 = (bf16[256,768]{1,0:T(8,128)(2,1)S(1)}, bf16[256,768]{1,0:T(8,128)(2,1)}, u32[]{:S(2)}) copy-start(bf16[256,768]{1,0:T(8,128)(2,1)} %param.15) | copy-start | bytes 1179652
  7.3 166.5 %all-gather.13.cloned.1.call-start = ((), (), s32[]{:S(2)}) async-start(), calls=%async_computation.4 | async-start | bytes 3538944 | tf_op jit(solution)/shard_map/all_gather | solution.py:76
  8.0 226.2 %all-gather.9.cloned.1.call-start = ((), (), s32[]{:S(2)}) async-start(), calls=%async_computation.2 | async-start | bytes 3538944 | tf_op jit(solution)/shard_map/all_gather | solution.py:74
  8.8 243.8 %reduce-scatter.3.cloned.1.call-start = ((), (), s32[]{:S(2)}) async-start(), calls=%async_computation.5 | async-start | bytes 3145728 | tf_op jit(solution)/shard_map/reduce_scatter | solution.py:92
  8.8 15.5 %collective-permute-start = (bf16[256,768]{1,0:T(8,128)(2,1)}, bf16[256,768]{1,0:T(8,128)(2,1)S(1)}, u32[]{:S(2)}, u32[]{:S(2)}) collective-permute-start(bf16[256,768]{1,0:T(8,128)(2,1)} %param.15), channel_id=1, source_target_pairs={{0,2},{2,4},{4,6},{6,8},{8,10},{10,12},{12,14},{14,0},{1,3},{3,5},... | collective-permute-start | bytes 1179656 | tf_op jit(solution)/shard_map/ppermute | solution.py:23
  24.3 22.5 %collective-permute-start.1 = (bf16[256,768]{1,0:T(8,128)(2,1)S(1)}, bf16[256,768]{1,0:T(8,128)(2,1)S(1)}, u32[]{:S(2)}, u32[]{:S(2)}) collective-permute-start(bf16[256,768]{1,0:T(8,128)(2,1)S(1)} %collective-permute-done), channel_id=1, source_target_pairs={{0,2},{2,4},{4,6},{6,8},{8,10},{10,12},{12,14},{14,0},{1,3},{3,5},... | collective-permute-start | bytes 1179656 | tf_op jit(solution)/shard_map/ppermute | solution.py:23
  24.3 24.6 %collective-permute-start.4 = (bf16[256,768]{1,0:T(8,128)(2,1)}, bf16[256,768]{1,0:T(8,128)(2,1)S(1)}, u32[]{:S(2)}, u32[]{:S(2)}) collective-permute-start(bf16[256,768]{1,0:T(8,128)(2,1)} %param.15), channel_id=1, source_target_pairs={{2,0},{4,2},{6,4},{8,6},{10,8},{12,10},{14,12},{0,14},{3,1},{5,3},... | collective-permute-start | bytes 1179656 | tf_op jit(solution)/shard_map/ppermute | solution.py:25
  46.8 25.0 %collective-permute-start.2 = (bf16[256,768]{1,0:T(8,128)(2,1)S(1)}, bf16[256,768]{1,0:T(8,128)(2,1)S(1)}, u32[]{:S(2)}, u32[]{:S(2)}) collective-permute-start(bf16[256,768]{1,0:T(8,128)(2,1)S(1)} %collective-permute-done.1), channel_id=1, source_target_pairs={{0,2},{2,4},{4,6},{6,8},{8,10},{10,12},{12,14},{14,0},{1,3},{3,5},... | collective-permute-start | bytes 1179656 | tf_op jit(solution)/shard_map/ppermute | solution.py:23
  48.9 33.4 %collective-permute-start.5 = (bf16[256,768]{1,0:T(8,128)(2,1)S(1)}, bf16[256,768]{1,0:T(8,128)(2,1)S(1)}, u32[]{:S(2)}, u32[]{:S(2)}) collective-permute-start(bf16[256,768]{1,0:T(8,128)(2,1)S(1)} %collective-permute-done.4), channel_id=1, source_target_pairs={{2,0},{4,2},{6,4},{8,6},{10,8},{12,10},{14,12},{0,14},{3,1},{5,3},... | collective-permute-start | bytes 1179656 | tf_op jit(solution)/shard_map/ppermute | solution.py:25
  71.8 24.4 %collective-permute-start.3 = (bf16[256,768]{1,0:T(8,128)(2,1)S(1)}, bf16[256,768]{1,0:T(8,128)(2,1)S(1)}, u32[]{:S(2)}, u32[]{:S(2)}) collective-permute-start(bf16[256,768]{1,0:T(8,128)(2,1)S(1)} %collective-permute-done.2), channel_id=1, source_target_pairs={{0,2},{2,4},{4,6},{6,8},{8,10},{10,12},{12,14},{14,0},{1,3},{3,5},... | collective-permute-start | bytes 1179656 | tf_op jit(solution)/shard_map/ppermute | solution.py:23
  82.2 19.5 %collective-permute-start.6 = (bf16[256,768]{1,0:T(8,128)(2,1)S(1)}, bf16[256,768]{1,0:T(8,128)(2,1)S(1)}, u32[]{:S(2)}, u32[]{:S(2)}) collective-permute-start(bf16[256,768]{1,0:T(8,128)(2,1)S(1)} %collective-permute-done.5), channel_id=1, source_target_pairs={{2,0},{4,2},{6,4},{8,6},{10,8},{12,10},{14,12},{0,14},{3,1},{5,3},... | collective-permute-start | bytes 1179656 | tf_op jit(solution)/shard_map/ppermute | solution.py:25
  102.5 6.9 copy-start
  109.4 3.9 copy-start.1
  234.2 9.9 %copy-start.5 = (bf16[2048]{0:T(1024)(128)(2,1)S(1)}, bf16[2048]{0:T(1024)(128)(2,1)}, u32[]{:S(2)}) copy-start(bf16[2048]{0:T(1024)(128)(2,1)} %param.18) | copy-start | bytes 12292
  244.0 23.6 %all-gather.15.cloned.1.call-start = ((), (), s32[]{:S(2)}) async-start(), calls=%async_computation.6 | async-start | bytes 3145728 | tf_op jit(solution)/shard_map/all_gather | solution.py:100
  255.6 139.7 %all-gather.17.cloned.1.call-start = ((), (), s32[]{:S(2)}) async-start(), calls=%async_computation.7 | async-start | bytes 9437184 | tf_op jit(solution)/shard_map/all_gather | solution.py:77
  256.2 263.9 %all-gather.19.cloned.1.call-start = ((), (), s32[]{:S(2)}) async-start(), calls=%async_computation.8 | async-start | bytes 9437184 | tf_op jit(solution)/shard_map/all_gather | solution.py:78
  257.0 388.3 %all-gather.21.cloned.1.call-start = ((), (), s32[]{:S(2)}) async-start(), calls=%async_computation.9 | async-start | bytes 9437184 | tf_op jit(solution)/shard_map/all_gather | solution.py:79
  257.7 413.1 %reduce-scatter.5.cloned.1.call-start = ((), (), s32[]{:S(2)}) async-start(), calls=%async_computation.10 | async-start | bytes 3145728 | tf_op jit(solution)/shard_map/reduce_scatter | solution.py:105
  267.6 377.7 %copy-start.6 = (bf16[512,2048]{1,0:T(8,128)(2,1)S(1)}, bf16[512,2048]{1,0:T(8,128)(2,1)}, u32[]{:S(2)}) copy-start(bf16[512,2048]{1,0:T(8,128)(2,1)} %all-gather.15.cloned.1.call-done) | copy-start | bytes 6291460
  662.8 22.7 %all-gather.23.cloned.1.call-start = ((), (), s32[]{:S(2)}) async-start(), calls=%async_computation.11 | async-start | bytes 3145728 | tf_op jit(solution)/shard_map/all_gather | solution.py:112
Sparse Core Ops, SparseCore 0:
  9.5 99.8 all-gather.10
  111.5 62.2 all-gather.12
  176.0 58.1 all-gather.8
  244.1 8.4 reduce-scatter.2
  255.8 11.8 all-gather.14
  269.6 125.6 all-gather.16
  397.4 122.6 all-gather.18
  522.2 123.1 all-gather.20
  662.9 7.8 reduce-scatter.4
  673.6 11.8 all-gather.22
